TPU v7x, 512 devices: a whole 4x4x16 slice. The times are simulated.
512 devices in a mesh: ep: 32 (over z, core), tp: 16 (over y, x).
Axes of the slice: x: 4, y: 4, z: 16, core: 2. Of those that a mesh axis runs over, the one named last changes fastest.
Arguments:
- attn_rows: bfloat16 [4096, 2048], P('ep'), may hold values from -6 to 6
- attn_gain: float32 [2048], replicated, may hold values from 0.1 to 1.9
- query_weight: bfloat16 [2048, 1024], P(None, 'tp'), may hold values from -0.125 to 0.125
- key_weight: bfloat16 [2048, 1024], P(None, 'tp'), may hold values from -0.125 to 0.125
- value_weight: bfloat16 [2048, 1024], P(None, 'tp'), may hold values from -0.125 to 0.125
- key_bias: bfloat16 [16, 4096], P('tp', 'ep'), may hold values from -14 to 0
- out_weight: bfloat16 [1024, 2048], P(None, 'tp'), may hold values from -0.75 to 0.75
- expert_rows: bfloat16 [4096, 2048], P('ep'), may hold values from -6 to 6
- expert_gain: float32 [2048], replicated, may hold values from 0.1 to 1.9
- expert_ids: int32 [4096, 2], P('ep'), may hold values from 0 to 31, all different within a row; in each aligned block of 128 rows (0 to 127, 128 to 255, ...) at most 16 rows name the same one
- group_logits: float32 [4096, 4], P('ep'), may hold values from -6 to 6
- pair_logits: float32 [4096, 2], P('ep'), may hold values from -6 to 6
- gate_weight: bfloat16 [32, 2048, 2048], P('ep', None, 'tp'), may hold values from -0.125 to 0.125
- up_weight: bfloat16 [32, 2048, 2048], P('ep', None, 'tp'), may hold values from -0.125 to 0.125
- down_weight: bfloat16 [32, 2048, 2048], P('ep', None, 'tp'), may hold values from -0.125 to 0.125
Outputs:
- mixed: bfloat16 [4096, 2048], P('ep', 'tp')
- expert_out: bfloat16 [4096, 2048], P('ep', 'tp')
Inputs may be any that keep to these rules, and one draw needn't show every extreme that they name: `expert_ids`: each row names two different experts; in every aligned block of 128 rows no expert is named more than 16 times.
All inputs are finite; a program needn't handle non-finite values.
Results may differ from a plain program's by a relative error of at most 0.0083.
Values may be sent and summed in bfloat16 or wider, within the bound.
No kernel may reach another device: no remote copies, remote signals or barrier semaphores. Data moves between devices by JAX's collectives and lax.ppermute only.
A program may use at most 64 MiB of HBM per device.

v0:
```python
import jax
import jax.numpy as jnp
from jax import lax
from jax.sharding import PartitionSpec as P

EXPERTS = 32
GROUPS = 4
GROUP_SIZE = 8
CAP = 16
epsilon = 1e-06


def sent_together(arrays, axis, dim, along):
    widths = [a.shape[along] for a in arrays]
    both = jnp.concatenate(arrays, axis=along)
    filled = lax.all_gather(both, axis, axis=dim, tiled=True)
    return tuple(jnp.split(filled, [sum(widths[:k]) for k in range(1, len(widths))], axis=along))


def laid_out(tiles, dim):
    lengths = list(tiles.shape[1:])
    lengths[dim] *= tiles.shape[0]
    return jnp.moveaxis(tiles, 0, dim).reshape(lengths)


def sent_to_all(shard, axis):
    copies = jnp.broadcast_to(shard, (lax.axis_size(axis), *shard.shape))
    return lax.all_to_all(copies, axis, split_axis=0, concat_axis=0, tiled=True)


def collect(shard, axis, dim):
    return laid_out(sent_to_all(shard, axis), dim)


def norm_rows(rows, gain):
    values = rows.astype(jnp.float32)
    scaled = values * lax.rsqrt(jnp.mean(values * values, axis=-1, keepdims=True) + epsilon)
    return (scaled * gain).astype(jnp.bfloat16)


def shards(
    attn_rows,
    attn_gain,
    query_weight,
    key_weight,
    value_weight,
    key_bias,
    out_weight,
    expert_rows,
    expert_gain,
    expert_ids,
    group_logits,
    pair_logits,
    gate_weight,
    up_weight,
    down_weight,
):
    rows_dev = attn_rows.shape[0]
    blocks = lax.axis_size("ep")
    own_start = lax.axis_index("ep") * rows_dev
    heads_local = key_bias.shape[0]
    head_size = query_weight.shape[1] // heads_local
    width_local = heads_local * head_size
    scale = head_size ** (-0.5)
    normed = norm_rows(attn_rows, attn_gain)
    query = jnp.dot(normed, query_weight, preferred_element_type=jnp.float32).astype(jnp.bfloat16)
    query = query.reshape(rows_dev, heads_local, head_size)
    keys = jnp.dot(normed, key_weight, preferred_element_type=jnp.float32).astype(jnp.bfloat16)
    values = jnp.dot(normed, value_weight, preferred_element_type=jnp.float32).astype(jnp.bfloat16)
    pairs = jnp.concatenate([keys, values], axis=1)
    bias_rows = key_bias.T
    query_pos = own_start + jnp.arange(rows_dev)
    init = (
        jnp.zeros((blocks, heads_local, rows_dev), jnp.float32),
        jnp.zeros((blocks, heads_local, rows_dev, head_size), jnp.float32),
    )
    piece = sent_together((pairs, bias_rows), "ep", 0, 1)

    def work(state):
        pair_rows, bias_piece = piece
        count = pair_rows.shape[0]
        spans = count // rows_dev
        key_part = pair_rows[:, :width_local].reshape(count, heads_local, head_size)
        value_part = pair_rows[:, width_local:].reshape(spans, rows_dev, heads_local, head_size)
        scores = (
            jnp.einsum("thd,shd->hts", query, key_part, preferred_element_type=jnp.float32) * scale
        )
        scores = scores + bias_piece.T.astype(jnp.float32)[:, None, :]
        scores = scores.reshape(heads_local, rows_dev, spans, rows_dev)
        causal = jnp.arange(count)[None, :] < query_pos[:, None]
        causal = causal.reshape(rows_dev, spans, rows_dev)
        negative_part = jax.nn.log_sigmoid(-scores)
        log_keep = jnp.where(causal, negative_part, 0.0)
        suffix = lax.cumsum(log_keep, axis=3, reverse=True) - log_keep
        weights = jnp.where(causal, jnp.exp(scores + negative_part + suffix), 0.0).astype(
            jnp.bfloat16
        )
        block_out = jnp.einsum(
            "htnr,nrhd->nhtd", weights, value_part, preferred_element_type=jnp.float32
        )
        block_keep = jnp.transpose(jnp.sum(log_keep, axis=3), (2, 0, 1))
        return (block_keep, block_out)

    def untouched(state):
        return state

    totals, outputs = lax.cond(jnp.int32(0) < own_start + rows_dev, work, untouched, init)
    later = lax.cumsum(totals, axis=0, reverse=True) - totals
    merged = jnp.sum(jnp.exp(later)[..., None] * outputs, axis=0)
    attended = jnp.transpose(merged, (1, 0, 2)).reshape(rows_dev, width_local).astype(jnp.bfloat16)
    mixed = jnp.dot(
        lax.all_gather(attended, "tp", axis=1, tiled=True),
        out_weight,
        preferred_element_type=jnp.float32,
    )
    mixed = mixed.astype(jnp.bfloat16)
    normed = norm_rows(expert_rows, expert_gain)
    width = normed.shape[1]
    cols_local = down_weight.shape[2]
    flattened = expert_ids.reshape(-1)
    picks = flattened.shape[0]
    marks = (flattened[:, None] == jnp.arange(EXPERTS)[None, :]).astype(jnp.int32)
    position = jnp.sum((jnp.cumsum(marks, axis=0) - marks) * marks, axis=1)
    source = jnp.arange(picks) // 2
    send = (
        jnp.zeros((EXPERTS, CAP, width), jnp.bfloat16).at[flattened, position].set(normed[source])
    )
    send = send.reshape(blocks, EXPERTS // blocks, CAP, width)
    shares = jnp.exp(group_logits)
    shares = shares / jnp.sum(shares, axis=1, keepdims=True)
    groups = expert_ids // GROUP_SIZE
    group_marks = (groups[:, :, None] == jnp.arange(GROUPS)[None, None, :]).astype(jnp.float32)
    chosen = jnp.sum(shares[:, None, :] * group_marks, axis=2)
    spread = pair_logits[:, 0] - pair_logits[:, 1]
    pair_share = jnp.stack([jax.nn.sigmoid(spread), jax.nn.sigmoid(-spread)], axis=1)
    route_weights = chosen * pair_share
    narrow = lax.dynamic_slice_in_dim(send, lax.axis_index("tp") * cols_local, cols_local, 3)
    add_piece = collect(
        lax.all_to_all(narrow, "ep", split_axis=0, concat_axis=0, tiled=True), "tp", 3
    )
    gate = jnp.einsum("secd,edf->secf", add_piece, gate_weight, preferred_element_type=jnp.float32)
    up = jnp.einsum("secd,edf->secf", add_piece, up_weight, preferred_element_type=jnp.float32)
    hidden = (jax.nn.silu(gate) * up).astype(jnp.bfloat16)
    result = jnp.einsum(
        "secf,efd->secd", collect(hidden, "tp", 3), down_weight, preferred_element_type=jnp.float32
    ).astype(jnp.bfloat16)
    back = lax.all_to_all(result, "ep", split_axis=0, concat_axis=0, tiled=True).reshape(
        EXPERTS, CAP, cols_local
    )
    picked = back[flattened, position].reshape(expert_rows.shape[0], 2, cols_local)
    combined = jnp.sum(route_weights[:, :, None] * picked.astype(jnp.float32), axis=1)
    expert_out = combined.astype(jnp.bfloat16)
    return (mixed, expert_out)


def solution(mesh):
    placed = (
        P("ep", None),
        P(),
        P(None, "tp"),
        P(None, "tp"),
        P(None, "tp"),
        P("tp", "ep"),
        P(None, "tp"),
        P("ep", None),
        P(),
        P("ep", None),
        P("ep", None),
        P("ep", None),
        P("ep", None, "tp"),
        P("ep", None, "tp"),
        P("ep", None, "tp"),
    )
    return jax.shard_map(
        shards,
        mesh=mesh,
        in_specs=placed,
        out_specs=(P("ep", "tp"), P("ep", "tp")),
        check_vma=False,
    )
```

profile of v0, /device:TPU:2, one launch (start us, length us, event | category | flops | bytes accessed | tf_op | source)
XLA Modules:
  0.0 225.2 jit_solution(5643384250437827587)
XLA Ops:
  7.2 0.8 copy.86
  8.0 0.1 eq.45
  8.2 0.1 eq.41
  8.3 0.1 reshape.361
  8.5 1.2 fusion.28
  9.7 0.6 reduce-window.6
  10.3 0.2 slice_reduce_fusion
  10.6 0.1 fusion.37
  10.7 1.2 fusion.30
  11.9 2.3 %gather_fusion = bf16[256,2048]{1,0:T(8,128)(2,1)} fusion(bf16[128,2048]{1,0:T(8,128)(2,1)S(1)} %fusion.30, s32[1024]{0:T(1024)S(1)} %pad_clamp_fusion), kind=kCustom, calls=%fused_computation | custom fusion | bytes 2098176 | tf_op jit(solution)/shard_map/gather | solution.py:126
  14.3 0.2 broadcast_in_dim.21
  14.5 33.3 %scatter_fusion = bf16[32,16,2048]{2,1,0:T(8,128)(2,1)S(1)} fusion(bf16[32,16,2048]{2,1,0:T(8,128)(2,1)S(1)} %broadcast_in_dim.21, s32[256]{0:T(256)S(1)} %bitcast.129, bf16[256,2048]{1,0:T(8,128)(2,1)} %gather_fusion), kind=kCustom, calls=%fused_computation.2 | custom fusion | bytes 3147776 | tf_op jit(solution)/shard_map/scatter | solution.py:126
  47.9 32.5 %all_to_all.23 = bf16[32,1,16,128]{3,2,1,0:T(8,128)(2,1)S(1)} all-to-all(bf16[32,1,16,128]{3,2,1,0:T(8,128)(2,1)S(1)} %dynamic-slice_bitcast_fusion), channel_id=1, replica_groups=mesh['ep'=32,'tp'=16] {'ep'}, dimensions={0} | all-to-all | bytes 262144 | tf_op jit(solution)/shard_map/all_to_all | solution.py:139
  80.3 1.8 broadcast_in_dim.22
  82.1 7.6 %all-to-all-start.1 = ((bf16[16,32,1,16,128]{4,3,1,2,0:T(8,128)(2,1)}), bf16[16,32,1,16,128]{4,3,1,2,0:T(8,128)(2,1)S(1)}, u32[]{:S(2)}, u32[]{:S(2)}) async-start(bf16[16,32,1,16,128]{4,3,1,2,0:T(8,128)(2,1)} %broadcast_in_dim.22), calls=%async_computation.1 | async-start | bytes 4194304 | tf_op jit(solution)/shard_map/all_to_all | solution.py:28
  89.8 0.2 fusion.25
  90.0 0.4 convolution_convert_fusion.3
  90.4 1.3 convolution_convert_fusion.4
  91.7 0.6 pad_maximum_fusion
  92.3 23.6 %all-to-all-done.1 = bf16[16,32,1,16,128]{4,3,1,2,0:T(8,128)(2,1)S(1)} async-done(((bf16[16,32,1,16,128]{4,3,1,2,0:T(8,128)(2,1)}), bf16[16,32,1,16,128]{4,3,1,2,0:T(8,128)(2,1)S(1)}, u32[]{:S(2)}, u32[]{:S(2)}) %all-to-all-start.1) | async-done | bytes 2097184 | tf_op jit(solution)/shard_map/all_to_all | solution.py:28
  115.9 3.8 %copy.90 = bf16[32,1,16,16,128]{4,3,2,0,1:T(8,128)(2,1)} copy(bf16[32,1,16,16,128]{4,2,0,1,3:T(8,128)(2,1)S(1)} %bitcast.131) | data formatting | bytes 4194304 | tf_op jit(solution)/shard_map/transpose | solution.py:23
  119.7 2.8 %reshape.363 = bf16[32,16,2048]{2,1,0:T(8,128)(2,1)S(1)} reshape(bf16[32,1,16,16,128]{4,3,2,0,1:T(8,128)(2,1)} %copy.90) | data formatting | bytes 4194304 | tf_op jit(solution)/shard_map/reshape.28
  122.6 0.7 convolution_bitcast_fusion.2
  123.3 0.3 copy-done.8
  123.6 0.7 fusion.23
  124.3 1.7 broadcast_in_dim.23
  126.0 8.0 %all-to-all-start.2 = ((bf16[16,32,1,16,128]{4,3,1,2,0:T(8,128)(2,1)}), bf16[16,32,1,16,128]{4,3,1,2,0:T(8,128)(2,1)}, u32[]{:S(2)}, u32[]{:S(2)}) async-start(bf16[16,32,1,16,128]{4,3,1,2,0:T(8,128)(2,1)} %broadcast_in_dim.23), calls=%async_computation.2 | async-start | bytes 4194304 | tf_op jit(solution)/shard_map/all_to_all | solution.py:28
  134.2 0.1 copy.85
  134.3 0.4 convolution_convert_fusion.2
  134.7 19.1 %all-gather.2.cloned.1.call-done = bf16[4096,129]{0,1:T(8,128)(2,1)} async-done(((bf16[128,129]{0,1:T(8,128)(2,1)}), bf16[4096,129]{0,1:T(8,128)(2,1)}) %all-gather.2.cloned.1.call-update) | async-done | bytes 1056784 | tf_op jit(solution)/shard_map/all_gather | solution.py:16
  153.8 19.2 %conditional.1 = (f32[32,1,128,64]{2,3,0,1:T(8,128)}, f32[32,1,128]{2,1,0:T(1,128)S(1)}) conditional(s32[]{:T(128)} %convert_element_type.82, () %tuple.16, (s32[]{:T(128)}, s32[128]{0:T(128)S(1)}, bf16[4096,129]{0,1:T(8,128)(2,1)}, bf16[128,64]{0,1:T(8,128)(2,1)S(1)}) %tuple.17), branch_computations={%region_1.0_spmd, %region_2.5_spmd} | conditional | flops 219160704 | bytes 19064852 | solution.py:107
  153.8 0.8 slice_convert_fusion
  154.7 1.5 fusion.11
  156.2 0.4 copy.97
  156.6 1.4 fusion.4
  158.1 2.4 %copy.79 = f32[128,32,128]{0,1,2:T(8,128)} copy(f32[128,32,128]{2,1,0:T(8,128)S(1)} %bitcast.128) | data formatting | bytes 4194304 | tf_op jit(solution)/shard_map/cond/branch_1_fun/reshape | solution.py:89
  160.5 9.9 %fusion.1 = bf16[128,32,128]{0,1,2:T(8,128)(2,1)S(1)} fusion(f32[128,32,128]{0,1,2:T(8,128)} %copy.79, s32[128]{0:T(128)S(1)} %broadcast_add_fusion, s32[32,128]{0,1:T(8,128)S(1)} %multiply_add_fusion), kind=kOutput, calls=%fused_computation.9 | output fusion | flops 78643200 | bytes 3162624 | tf_op jit(solution)/shard_map/cond/branch_1_fun/reduce_window_sum | solution.py:94
  170.4 2.6 %convolution_bitcast_fusion = f32[32,1,128,64]{2,3,0,1:T(8,128)} fusion(bf16[128,32,128]{0,1,2:T(8,128)(2,1)S(1)} %fusion.1, bf16[4096,129]{0,1:T(8,128)(2,1)} %get-tuple-element.17), kind=kOutput, calls=%fused_computation.22 | convolution fusion | flops 67108864 | bytes 2621440 | tf_op jit(solution)/shard_map/cond/branch_1_fun/htnr,nrhd->nhtd/dot_general | solution.py:98
  173.0 4.0 %copy.91 = bf16[32,1,16,16,128]{4,3,2,0,1:T(8,128)(2,1)S(1)} copy(bf16[32,1,16,16,128]{4,2,0,1,3:T(8,128)(2,1)} %bitcast.26) | data formatting | bytes 4194304 | tf_op jit(solution)/shard_map/transpose | solution.py:23
  177.0 2.3 %reshape.366 = bf16[32,16,2048]{2,1,0:T(8,128)(2,1)} reshape(bf16[32,1,16,16,128]{4,3,2,0,1:T(8,128)(2,1)S(1)} %copy.91) | data formatting | bytes 4194304 | tf_op jit(solution)/shard_map/reshape.35
  179.4 3.0 %fusion.22 = bf16[32,1,16,128]{3,2,1,0:T(8,128)(2,1)} fusion(bf16[32,16,2048]{2,1,0:T(8,128)(2,1)} %reshape.366, bf16[1,2048,128]{2,1,0:T(8,128)(2,1)S(1)} %copy-done.2), kind=kOutput, calls=%fused_computation.44 | convolution fusion | flops 268500992 | bytes 2752512 | tf_op jit(solution)/shard_map/secf,efd->secd/dot_general | solution.py:144
  182.4 7.3 %all-to-all-start.3 = ((bf16[32,1,16,128]{3,2,1,0:T(8,128)(2,1)}), bf16[32,1,16,128]{3,2,1,0:T(8,128)(2,1)S(1)}, u32[]{:S(2)}, u32[]{:S(2)}) async-start(bf16[32,1,16,128]{3,2,1,0:T(8,128)(2,1)} %fusion.22), calls=%async_computation.3 | async-start | bytes 262144 | tf_op jit(solution)/shard_map/all_to_all | solution.py:147
  189.7 0.1 fusion.24
  189.8 1.3 multiply_reduce_fusion
  191.1 23.8 %all_gather.7 = bf16[128,1024]{0,1:T(8,128)(2,1)S(1)} all-gather(bf16[128,64]{0,1:T(8,128)(2,1)S(1)} %multiply_reduce_fusion), channel_id=1, replica_groups=mesh['ep'=32,'tp'=16] {'tp'}, dimensions={1}, use_global_device_ids=true | all-gather | bytes 278528 | tf_op jit(solution)/shard_map/all_gather | solution.py:112
  214.9 0.9 convolution_convert_fusion.1
  215.8 1.7 gather_fusion.1
  217.5 0.9 fusion.34
  (47 shorter events, 0.5 us)
Async XLA Ops:
  7.2 115.4 %copy-start = (bf16[1,2048,128]{2,1,0:T(8,128)(2,1)S(1)}, bf16[1,2048,128]{2,1,0:T(8,128)(2,1)}, u32[]{:S(2)}) copy-start(bf16[1,2048,128]{2,1,0:T(8,128)(2,1)} %param.29) | copy-start | bytes 1572868
  82.1 7.7 %copy-start.1 = (bf16[128,2048]{1,0:T(8,128)(2,1)S(1)}, bf16[128,2048]{1,0:T(8,128)(2,1)}, u32[]{:S(2)}) copy-start(bf16[128,2048]{1,0:T(8,128)(2,1)} %param.17) | copy-start | bytes 1572868
  82.1 7.9 %copy-start.9 = (bf16[2048,64]{0,1:T(8,128)(2,1)S(1)}, bf16[2048,64]{0,1:T(8,128)(2,1)}, u32[]{:S(2)}) copy-start(bf16[2048,64]{0,1:T(8,128)(2,1)} %param.21) | copy-start | bytes 786436
  82.1 7.9 %copy-start.11 = (f32[2048]{0:T(1024)S(1)}, f32[2048]{0:T(1024)}, u32[]{:S(2)}) copy-start(f32[2048]{0:T(1024)} %param.18) | copy-start | bytes 24580
  82.1 33.8 %all-to-all-start.1 = ((bf16[16,32,1,16,128]{4,3,1,2,0:T(8,128)(2,1)}), bf16[16,32,1,16,128]{4,3,1,2,0:T(8,128)(2,1)S(1)}, u32[]{:S(2)}, u32[]{:S(2)}) async-start(bf16[16,32,1,16,128]{4,3,1,2,0:T(8,128)(2,1)} %broadcast_in_dim.22), calls=%async_computation.1 | async-start | bytes 4194304 | tf_op jit(solution)/shard_map/all_to_all | solution.py:28
  89.7 2.0 copy-start.7
  89.7 64.1 %all-gather.2.cloned.1.call-start = ((), (), s32[]{:S(2)}) async-start(), calls=%async_computation.4 | async-start | bytes 1148928 | tf_op jit(solution)/shard_map/all_gather | solution.py:16
  122.5 1.0 copy-start.8
  126.0 8.0 %copy-start.4 = (f32[128,4]{0,1:T(4,128)S(1)}, f32[128,4]{0,1:T(4,128)}, u32[]{:S(2)}) copy-start(f32[128,4]{0,1:T(4,128)} %param.27) | copy-start | bytes 6148
  126.0 8.1 %copy-start.5 = (s32[128,2]{0,1:T(2,128)S(1)}, s32[128,2]{0,1:T(2,128)}, u32[]{:S(2)}) copy-start(s32[128,2]{0,1:T(2,128)} %param.26) | copy-start | bytes 3076
  126.0 8.1 %copy-start.6 = (f32[128,2]{0,1:T(2,128)S(1)}, f32[128,2]{0,1:T(2,128)}, u32[]{:S(2)}) copy-start(f32[128,2]{0,1:T(2,128)} %param.28) | copy-start | bytes 3076
  126.0 8.3 %copy-start.10 = (bf16[2048,64]{0,1:T(8,128)(2,1)S(1)}, bf16[2048,64]{0,1:T(8,128)(2,1)}, u32[]{:S(2)}) copy-start(bf16[2048,64]{0,1:T(8,128)(2,1)} %param.19) | copy-start | bytes 786436
  126.0 47.0 %all-to-all-start.2 = ((bf16[16,32,1,16,128]{4,3,1,2,0:T(8,128)(2,1)}), bf16[16,32,1,16,128]{4,3,1,2,0:T(8,128)(2,1)}, u32[]{:S(2)}, u32[]{:S(2)}) async-start(bf16[16,32,1,16,128]{4,3,1,2,0:T(8,128)(2,1)} %broadcast_in_dim.23), calls=%async_computation.2 | async-start | bytes 4194304 | tf_op jit(solution)/shard_map/all_to_all | solution.py:28
  177.0 2.3 %copy-start.2 = (bf16[1,2048,128]{2,1,0:T(8,128)(2,1)S(1)}, bf16[1,2048,128]{2,1,0:T(8,128)(2,1)}, u32[]{:S(2)}) copy-start(bf16[1,2048,128]{2,1,0:T(8,128)(2,1)} %param.31) | copy-start | bytes 1572868
  179.4 35.5 %copy-start.3 = (bf16[1024,128]{1,0:T(8,128)(2,1)S(1)}, bf16[1024,128]{1,0:T(8,128)(2,1)}, u32[]{:S(2)}) copy-start(bf16[1024,128]{1,0:T(8,128)(2,1)} %param.23) | copy-start | bytes 786436
  182.4 33.4 %all-to-all-start.3 = ((bf16[32,1,16,128]{3,2,1,0:T(8,128)(2,1)}), bf16[32,1,16,128]{3,2,1,0:T(8,128)(2,1)S(1)}, u32[]{:S(2)}, u32[]{:S(2)}) async-start(bf16[32,1,16,128]{3,2,1,0:T(8,128)(2,1)} %fusion.22), calls=%async_computation.3 | async-start | bytes 262144 | tf_op jit(solution)/shard_map/all_to_all | solution.py:147
Sparse Core Ops, SparseCore 0:
  92.6 61.1 all-gather.1
where the time goes:
time: 227 us; the launch traced here: 225 us
  local copies, waits for them, and re-layouts  58.8 us (26%)
  blocking collectives  56.3 us (25%)
  waiting for transfers between devices  42.7 us (19%)
  starting transfers between devices  23 us (10%)
  other arithmetic  18.6 us (8%)
  between operations  14.3 us (6%)
  matrix products  11.5 us (5%)
    scatter x1, local copies, waits for them, and re-layouts, shards(): jnp.zeros((EXPERTS, CAP, width), jnp.bfloat16).at[flattened, position]  33.3 us
    all_to_all x1, blocking collectives, shards(): lax.all_to_all(narrow, 'ep', split_axis=0, concat_axis=0, tiled=True)  32.5 us
    all_gather x1, blocking collectives, shards(): lax.all_gather(attended, 'tp', axis=1, tiled=True)  23.8 us
    all_to_all x2, waiting for transfers between devices, sent_to_all(): return lax.all_to_all(copies, axis, split_axis=0, concat_axis=0, tiled=True)  23.6 us
    all_gather x1, waiting for transfers between devices, sent_together(): filled = lax.all_gather(both, axis, axis=dim, tiled=True)  19.1 us
    all_to_all x2, starting transfers between devices, sent_to_all(): return lax.all_to_all(copies, axis, split_axis=0, concat_axis=0, tiled=True)  15.6 us
    another operation x1, other arithmetic, work(): suffix = lax.cumsum(log_keep, axis=3, reverse=True) - log_keep  9.92 us
    transpose x2, local copies, waits for them, and re-layouts, laid_out(): return jnp.moveaxis(tiles, 0, dim).reshape(lengths)  7.81 us
  transfers between devices with their start and end apart: 4, of which 2 were waited for; matrix products, arithmetic and copies ran while one was open for 15% of the time, Pallas kernels for 0%

commit v1 on v0

--- a/solution.py
+++ b/solution.py
@@ -8,6 +8,19 @@
 GROUP_SIZE = 8
 CAP = 16
 epsilon = 1e-06
+
+
+def ring_gather(shard, axis, dim):
+    ways = lax.axis_size(axis)
+    up = [(d, (d + 1) % ways) for d in range(ways)]
+    down = [(d, (d - 1) % ways) for d in range(ways)]
+    earlier, later = ([shard], [shard])
+    for _ in range(ways // 2):
+        earlier.append(lax.ppermute(earlier[-1], axis, up))
+    for _ in range((ways - 1) // 2):
+        later.append(lax.ppermute(later[-1], axis, down))
+    line = jnp.concatenate([*earlier[::-1], *later[1:]], axis=dim)
+    return jnp.roll(line, (lax.axis_index(axis) - ways // 2) * shard.shape[dim], axis=dim)
 
 
 def sent_together(arrays, axis, dim, along):
@@ -108,11 +121,7 @@
     later = lax.cumsum(totals, axis=0, reverse=True) - totals
     merged = jnp.sum(jnp.exp(later)[..., None] * outputs, axis=0)
     attended = jnp.transpose(merged, (1, 0, 2)).reshape(rows_dev, width_local).astype(jnp.bfloat16)
-    mixed = jnp.dot(
-        lax.all_gather(attended, "tp", axis=1, tiled=True),
-        out_weight,
-        preferred_element_type=jnp.float32,
-    )
+    mixed = jnp.dot(ring_gather(attended, "tp", 1), out_weight, preferred_element_type=jnp.float32)
     mixed = mixed.astype(jnp.bfloat16)
     normed = norm_rows(expert_rows, expert_gain)
     width = normed.shape[1]

time: 227 us -> 290 us (1.28)
  the two profiles are of different devices: /device:TPU:2 before, /device:TPU:1 now
where the time goes in v1:
time: 290 us; the launch traced here: 288 us
  starting transfers between devices  106 us (37%)
  waiting for transfers between devices  72.4 us (25%)
  local copies, waits for them, and re-layouts  64 us (22%)
  other arithmetic  17.7 us (6%)
  between operations  15 us (5%)
  matrix products  13.1 us (5%)
    ppermute x7, starting transfers between devices, ring_gather(): later.append(lax.ppermute(later[-1], axis, down))  46.8 us
    scatter x1, local copies, waits for them, and re-layouts, shards(): jnp.zeros((EXPERTS, CAP, width), jnp.bfloat16).at[flattened, position]  33.3 us
    all_to_all x2, waiting for transfers between devices, sent_to_all(): return lax.all_to_all(copies, axis, split_axis=0, concat_axis=0, tiled=True)  22.3 us
    all_gather x1, waiting for transfers between devices, sent_together(): filled = lax.all_gather(both, axis, axis=dim, tiled=True)  21.1 us
    ppermute x8, starting transfers between devices, ring_gather(): earlier.append(lax.ppermute(earlier[-1], axis, up))  16.8 us
    all_to_all x1, starting transfers between devices, shards(): lax.all_to_all(narrow, 'ep', split_axis=0, concat_axis=0, tiled=True)  16.7 us
    all_to_all x1, starting transfers between devices, shards(): lax.all_to_all(result, 'ep', split_axis=0, concat_axis=0, tiled=True)  15.6 us
    ppermute x7, waiting for transfers between devices, ring_gather(): later.append(lax.ppermute(later[-1], axis, down))  13.6 us
  transfers between devices with their start and end apart: 20, of which 5 were waited for; matrix products, arithmetic and copies ran while one was open for 27% of the time, Pallas kernels for 0%

profile of v1, /device:TPU:1, one launch (start us, length us, event | category | flops | bytes accessed | tf_op | source)
XLA Modules:
  0.0 288.2 jit_solution(18312590891655294601)
XLA Ops:
  7.3 1.3 fusion.25
  8.6 1.5 convolution_convert_fusion.3
  10.1 1.5 convolution_convert_fusion.4
  14.1 2.4 gather_fusion
  16.8 33.3 %scatter_fusion = bf16[32,16,2048]{2,1,0:T(8,128)(2,1)S(1)} fusion(bf16[32,16,2048]{2,1,0:T(8,128)(2,1)S(1)} %broadcast_in_dim.21, s32[256]{0:T(256)S(1)} %bitcast.128, bf16[256,2048]{1,0:T(8,128)(2,1)} %gather_fusion), kind=kCustom, calls=%fused_computation.2 | custom fusion | bytes 3147776 | tf_op jit(solution)/shard_map/scatter | solution.py:135
  50.8 16.7 %all-to-all-start = ((bf16[32,1,16,128]{3,2,1,0:T(8,128)(2,1)}), bf16[32,1,16,128]{3,2,1,0:T(8,128)(2,1)S(1)}, u32[]{:S(2)}, u32[]{:S(2)}) async-start(bf16[32,1,16,128]{3,2,1,0:T(8,128)(2,1)} %dynamic-slice_bitcast_fusion), calls=%async_computation | async-start | bytes 262144 | tf_op jit(solution)/shard_map/all_to_all | solution.py:148
  67.6 1.3 convolution_convert_fusion.2
  68.9 21.1 %all-gather.2.cloned.1.call-done = bf16[4096,129]{0,1:T(8,128)(2,1)} async-done(((bf16[128,129]{0,1:T(8,128)(2,1)}), bf16[4096,129]{0,1:T(8,128)(2,1)}) %all-gather.2.cloned.1.call-update) | async-done | bytes 1056784 | tf_op jit(solution)/shard_map/all_gather | solution.py:29
  90.0 19.2 %conditional.1 = (f32[32,1,128,64]{2,3,0,1:T(8,128)}, f32[32,1,128]{2,1,0:T(1,128)S(1)}) conditional(s32[]{:T(128)} %convert_element_type.82, () %tuple.16, (s32[]{:T(128)}, s32[128]{0:T(128)S(1)}, bf16[4096,129]{0,1:T(8,128)(2,1)}, bf16[128,64]{0,1:T(8,128)(2,1)S(1)}) %tuple.17), branch_computations={%region_1.0_spmd, %region_2.5_spmd} | conditional | flops 219160704 | bytes 19064852 | solution.py:120
  91.0 1.5 fusion.11
  92.9 1.4 fusion.4
  94.4 2.4 copy.79
  96.7 9.9 %fusion.1 = bf16[128,32,128]{0,1,2:T(8,128)(2,1)S(1)} fusion(f32[128,32,128]{0,1,2:T(8,128)} %copy.79, s32[128]{0:T(128)S(1)} %broadcast_add_fusion, s32[32,128]{0,1:T(8,128)S(1)} %multiply_add_fusion), kind=kOutput, calls=%fused_computation.9 | output fusion | flops 78643200 | bytes 3162624 | tf_op jit(solution)/shard_map/cond/branch_1_fun/reduce_window_sum | solution.py:107
  106.7 2.6 convolution_bitcast_fusion
  109.4 1.3 multiply_reduce_fusion
  110.7 3.2 %collective-permute-start = (bf16[128,64]{0,1:T(8,128)(2,1)S(1)}, bf16[128,64]{0,1:T(8,128)(2,1)S(1)}, u32[]{:S(2)}, u32[]{:S(2)}) collective-permute-start(bf16[128,64]{0,1:T(8,128)(2,1)S(1)} %multiply_reduce_fusion), channel_id=1, source_target_pairs={{0,1},{1,2},{2,3},{3,4},{4,5},{5,6},{6,7},{7,8},{8,9},{9,10},{10,1... | collective-permute-start | bytes 49160 | tf_op jit(solution)/shard_map/ppermute | solution.py:19
  113.9 4.6 %collective-permute-done = bf16[128,64]{0,1:T(8,128)(2,1)S(1)} collective-permute-done((bf16[128,64]{0,1:T(8,128)(2,1)S(1)}, bf16[128,64]{0,1:T(8,128)(2,1)S(1)}, u32[]{:S(2)}, u32[]{:S(2)}) %collective-permute-start) | collective-permute-done | bytes 16416 | tf_op jit(solution)/shard_map/ppermute | solution.py:19
  118.5 2.1 collective-permute-start.1
  120.6 6.7 %collective-permute-start.8 = (bf16[128,64]{0,1:T(8,128)(2,1)S(1)}, bf16[128,64]{0,1:T(8,128)(2,1)S(1)}, u32[]{:S(2)}, u32[]{:S(2)}) collective-permute-start(bf16[128,64]{0,1:T(8,128)(2,1)S(1)} %multiply_reduce_fusion), channel_id=1, source_target_pairs={{0,15},{1,0},{2,1},{3,2},{4,3},{5,4},{6,5},{7,6},{8,7},{9,8},{10,9... | collective-permute-start | bytes 49160 | tf_op jit(solution)/shard_map/ppermute | solution.py:21
  127.3 1.9 collective-permute-start.2
  129.3 6.7 %collective-permute-start.9 = (bf16[128,64]{0,1:T(8,128)(2,1)S(1)}, bf16[128,64]{0,1:T(8,128)(2,1)S(1)}, u32[]{:S(2)}, u32[]{:S(2)}) collective-permute-start(bf16[128,64]{0,1:T(8,128)(2,1)S(1)} %collective-permute-done.8), channel_id=1, source_target_pairs={{0,15},{1,0},{2,1},{3,2},{4,3},{5,4},{6,5},{7,6},{8,7},{9,8},{10,9... | collective-permute-start | bytes 49160 | tf_op jit(solution)/shard_map/ppermute | solution.py:21
  136.0 1.9 collective-permute-start.3
  138.0 1.7 broadcast_in_dim.22
  139.7 6.3 %all-to-all-start.1 = ((bf16[16,32,1,16,128]{4,3,1,2,0:T(8,128)(2,1)}), bf16[16,32,1,16,128]{4,3,1,2,0:T(8,128)(2,1)S(1)}, u32[]{:S(2)}, u32[]{:S(2)}) async-start(bf16[16,32,1,16,128]{4,3,1,2,0:T(8,128)(2,1)} %broadcast_in_dim.22), calls=%async_computation.1 | async-start | bytes 4194304 | tf_op jit(solution)/shard_map/all_to_all | solution.py:41
  146.0 6.6 %collective-permute-start.10 = (bf16[128,64]{0,1:T(8,128)(2,1)S(1)}, bf16[128,64]{0,1:T(8,128)(2,1)S(1)}, u32[]{:S(2)}, u32[]{:S(2)}) collective-permute-start(bf16[128,64]{0,1:T(8,128)(2,1)S(1)} %collective-permute-done.9), channel_id=1, source_target_pairs={{0,15},{1,0},{2,1},{3,2},{4,3},{5,4},{6,5},{7,6},{8,7},{9,8},{10,9... | collective-permute-start | bytes 49160 | tf_op jit(solution)/shard_map/ppermute | solution.py:21
  152.6 1.9 collective-permute-start.4
  154.6 13.5 %collective-permute-done.10 = bf16[128,64]{0,1:T(8,128)(2,1)S(1)} collective-permute-done((bf16[128,64]{0,1:T(8,128)(2,1)S(1)}, bf16[128,64]{0,1:T(8,128)(2,1)S(1)}, u32[]{:S(2)}, u32[]{:S(2)}) %collective-permute-start.10) | collective-permute-done | bytes 16416 | tf_op jit(solution)/shard_map/ppermute | solution.py:21
  168.1 6.7 %collective-permute-start.11 = (bf16[128,64]{0,1:T(8,128)(2,1)S(1)}, bf16[128,64]{0,1:T(8,128)(2,1)S(1)}, u32[]{:S(2)}, u32[]{:S(2)}) collective-permute-start(bf16[128,64]{0,1:T(8,128)(2,1)S(1)} %collective-permute-done.10), channel_id=1, source_target_pairs={{0,15},{1,0},{2,1},{3,2},{4,3},{5,4},{6,5},{7,6},{8,7},{9,8},{10,9... | collective-permute-start | bytes 49160 | tf_op jit(solution)/shard_map/ppermute | solution.py:21
  174.9 1.9 collective-permute-start.5
  176.9 6.7 %collective-permute-start.12 = (bf16[128,64]{0,1:T(8,128)(2,1)S(1)}, bf16[128,64]{0,1:T(8,128)(2,1)S(1)}, u32[]{:S(2)}, u32[]{:S(2)}) collective-permute-start(bf16[128,64]{0,1:T(8,128)(2,1)S(1)} %collective-permute-done.11), channel_id=1, source_target_pairs={{0,15},{1,0},{2,1},{3,2},{4,3},{5,4},{6,5},{7,6},{8,7},{9,8},{10,9... | collective-permute-start | bytes 49160 | tf_op jit(solution)/shard_map/ppermute | solution.py:21
  183.6 1.9 collective-permute-start.6
  185.6 6.7 %collective-permute-start.13 = (bf16[128,64]{0,1:T(8,128)(2,1)S(1)}, bf16[128,64]{0,1:T(8,128)(2,1)}, u32[]{:S(2)}, u32[]{:S(2)}) collective-permute-start(bf16[128,64]{0,1:T(8,128)(2,1)S(1)} %collective-permute-done.12), channel_id=1, source_target_pairs={{0,15},{1,0},{2,1},{3,2},{4,3},{5,4},{6,5},{7,6},{8,7},{9,8},{10,9... | collective-permute-start | bytes 49160 | tf_op jit(solution)/shard_map/ppermute | solution.py:21
  192.3 1.9 collective-permute-start.7
  194.4 6.7 %collective-permute-start.14 = (bf16[128,64]{0,1:T(8,128)(2,1)}, bf16[128,64]{0,1:T(8,128)(2,1)}, u32[]{:S(2)}, u32[]{:S(2)}) collective-permute-start(bf16[128,64]{0,1:T(8,128)(2,1)} %collective-permute-done.13), channel_id=1, source_target_pairs={{0,15},{1,0},{2,1},{3,2},{4,3},{5,4},{6,5},{7,6},{8,7},{9,8},{10,9... | collective-permute-start | bytes 49160 | tf_op jit(solution)/shard_map/ppermute | solution.py:21
  201.2 3.8 %copy.90 = bf16[32,1,16,16,128]{4,3,2,0,1:T(8,128)(2,1)} copy(bf16[32,1,16,16,128]{4,2,0,1,3:T(8,128)(2,1)S(1)} %bitcast.130) | data formatting | bytes 4194304 | tf_op jit(solution)/shard_map/transpose | solution.py:36
  205.1 2.8 reshape.363
  209.7 1.7 broadcast_in_dim.23
  211.5 3.9 %all-to-all-start.2 = ((bf16[16,32,1,16,128]{4,3,1,2,0:T(8,128)(2,1)}), bf16[16,32,1,16,128]{4,3,1,2,0:T(8,128)(2,1)S(1)}, u32[]{:S(2)}, u32[]{:S(2)}) async-start(bf16[16,32,1,16,128]{4,3,1,2,0:T(8,128)(2,1)} %broadcast_in_dim.23), calls=%async_computation.2 | async-start | bytes 4194304 | tf_op jit(solution)/shard_map/all_to_all | solution.py:41
  217.1 22.3 %all-to-all-done.2 = bf16[16,32,1,16,128]{4,3,1,2,0:T(8,128)(2,1)S(1)} async-done(((bf16[16,32,1,16,128]{4,3,1,2,0:T(8,128)(2,1)}), bf16[16,32,1,16,128]{4,3,1,2,0:T(8,128)(2,1)S(1)}, u32[]{:S(2)}, u32[]{:S(2)}) %all-to-all-start.2) | async-done | bytes 2097184 | tf_op jit(solution)/shard_map/all_to_all | solution.py:41
  239.4 3.8 %copy.91 = bf16[32,1,16,16,128]{4,3,2,0,1:T(8,128)(2,1)} copy(bf16[32,1,16,16,128]{4,2,0,1,3:T(8,128)(2,1)S(1)} %bitcast.131) | data formatting | bytes 4194304 | tf_op jit(solution)/shard_map/transpose | solution.py:36
  243.1 2.9 reshape.366
  246.0 1.4 fusion.22
  247.4 15.6 %all-to-all-start.3 = ((bf16[32,1,16,128]{3,2,1,0:T(8,128)(2,1)}), bf16[32,1,16,128]{3,2,1,0:T(8,128)(2,1)S(1)}, u32[]{:S(2)}, u32[]{:S(2)}) async-start(bf16[32,1,16,128]{3,2,1,0:T(8,128)(2,1)} %fusion.22), calls=%async_computation.3 | async-start | bytes 262144 | tf_op jit(solution)/shard_map/all_to_all | solution.py:156
  263.6 1.3 constant_dynamic-update-slice_fusion.1
  264.9 1.3 constant_dynamic-update-slice_fusion
  266.2 1.8 convolution_convert_fusion.1
  268.1 10.8 %all-to-all-done.3 = bf16[32,1,16,128]{3,2,1,0:T(8,128)(2,1)S(1)} async-done(((bf16[32,1,16,128]{3,2,1,0:T(8,128)(2,1)}), bf16[32,1,16,128]{3,2,1,0:T(8,128)(2,1)S(1)}, u32[]{:S(2)}, u32[]{:S(2)}) %all-to-all-start.3) | async-done | bytes 131104 | tf_op jit(solution)/shard_map/all_to_all | solution.py:156
  278.8 1.7 gather_fusion.1
  (153 shorter events, 10.2 us)
Async XLA Ops:
  7.2 200.7 %copy-start = (bf16[1,2048,128]{2,1,0:T(8,128)(2,1)S(1)}, bf16[1,2048,128]{2,1,0:T(8,128)(2,1)}, u32[]{:S(2)}) copy-start(bf16[1,2048,128]{2,1,0:T(8,128)(2,1)} %param.29) | copy-start | bytes 1572868
  7.2 4.4 %copy-start.31 = (bf16[1,128]{1,0:T(2,128)(2,1)S(1)}, bf16[1,128]{1,0:T(2,128)(2,1)}, u32[]{:S(2)}) copy-start(bf16[1,128]{1,0:T(2,128)(2,1)} %param.22) | copy-start | bytes 772
  7.2 5.0 %copy-start.29 = (s32[128,2]{0,1:T(2,128)S(1)}, s32[128,2]{0,1:T(2,128)}, u32[]{:S(2)}) copy-start(s32[128,2]{0,1:T(2,128)} %param.26) | copy-start | bytes 3076
  7.2 6.5 %copy-start.1 = (bf16[128,2048]{1,0:T(8,128)(2,1)S(1)}, bf16[128,2048]{1,0:T(8,128)(2,1)}, u32[]{:S(2)}) copy-start(bf16[128,2048]{1,0:T(8,128)(2,1)} %param.24) | copy-start | bytes 1572868
  7.2 6.7 %copy-start.27 = (f32[2048]{0:T(1024)S(1)}, f32[2048]{0:T(1024)}, u32[]{:S(2)}) copy-start(f32[2048]{0:T(1024)} %param.25) | copy-start | bytes 24580
  7.2 82.8 %all-gather.2.cloned.1.call-start = ((), (), s32[]{:S(2)}) async-start(), calls=%async_computation.4 | async-start | bytes 1148928 | tf_op jit(solution)/shard_map/all_gather | solution.py:29
  16.8 50.8 %copy-start.2 = (bf16[128,2048]{1,0:T(8,128)(2,1)S(1)}, bf16[128,2048]{1,0:T(8,128)(2,1)}, u32[]{:S(2)}) copy-start(bf16[128,2048]{1,0:T(8,128)(2,1)} %param.17) | copy-start | bytes 1572868
  16.8 50.8 %copy-start.33 = (f32[2048]{0:T(1024)S(1)}, f32[2048]{0:T(1024)}, u32[]{:S(2)}) copy-start(f32[2048]{0:T(1024)} %param.18) | copy-start | bytes 24580
  50.8 87.2 %all-to-all-start = ((bf16[32,1,16,128]{3,2,1,0:T(8,128)(2,1)}), bf16[32,1,16,128]{3,2,1,0:T(8,128)(2,1)S(1)}, u32[]{:S(2)}, u32[]{:S(2)}) async-start(bf16[32,1,16,128]{3,2,1,0:T(8,128)(2,1)} %dynamic-slice_bitcast_fusion), calls=%async_computation | async-start | bytes 262144 | tf_op jit(solution)/shard_map/all_to_all | solution.py:148
  90.0 39.2 %copy-start.28 = (f32[128,4]{0,1:T(4,128)S(1)}, f32[128,4]{0,1:T(4,128)}, u32[]{:S(2)}) copy-start(f32[128,4]{0,1:T(4,128)} %param.27) | copy-start | bytes 6148
  110.7 7.8 %collective-permute-start = (bf16[128,64]{0,1:T(8,128)(2,1)S(1)}, bf16[128,64]{0,1:T(8,128)(2,1)S(1)}, u32[]{:S(2)}, u32[]{:S(2)}) collective-permute-start(bf16[128,64]{0,1:T(8,128)(2,1)S(1)} %multiply_reduce_fusion), channel_id=1, source_target_pairs={{0,1},{1,2},{2,3},{3,4},{4,5},{5,6},{6,7},{7,8},{8,9},{9,10},{10,1... | collective-permute-start | bytes 49160 | tf_op jit(solution)/shard_map/ppermute | solution.py:19
  118.5 8.8 %collective-permute-start.1 = (bf16[128,64]{0,1:T(8,128)(2,1)S(1)}, bf16[128,64]{0,1:T(8,128)(2,1)S(1)}, u32[]{:S(2)}, u32[]{:S(2)}) collective-permute-start(bf16[128,64]{0,1:T(8,128)(2,1)S(1)} %collective-permute-done), channel_id=1, source_target_pairs={{0,1},{1,2},{2,3},{3,4},{4,5},{5,6},{6,7},{7,8},{8,9},{9,10},{10,1... | collective-permute-start | bytes 49160 | tf_op jit(solution)/shard_map/ppermute | solution.py:19
  120.6 8.7 %collective-permute-start.8 = (bf16[128,64]{0,1:T(8,128)(2,1)S(1)}, bf16[128,64]{0,1:T(8,128)(2,1)S(1)}, u32[]{:S(2)}, u32[]{:S(2)}) collective-permute-start(bf16[128,64]{0,1:T(8,128)(2,1)S(1)} %multiply_reduce_fusion), channel_id=1, source_target_pairs={{0,15},{1,0},{2,1},{3,2},{4,3},{5,4},{6,5},{7,6},{8,7},{9,8},{10,9... | collective-permute-start | bytes 49160 | tf_op jit(solution)/shard_map/ppermute | solution.py:21
  127.3 8.7 %collective-permute-start.2 = (bf16[128,64]{0,1:T(8,128)(2,1)S(1)}, bf16[128,64]{0,1:T(8,128)(2,1)S(1)}, u32[]{:S(2)}, u32[]{:S(2)}) collective-permute-start(bf16[128,64]{0,1:T(8,128)(2,1)S(1)} %collective-permute-done.1), channel_id=1, source_target_pairs={{0,1},{1,2},{2,3},{3,4},{4,5},{5,6},{6,7},{7,8},{8,9},{9,10},{10,1... | collective-permute-start | bytes 49160 | tf_op jit(solution)/shard_map/ppermute | solution.py:19
  129.3 16.7 %collective-permute-start.9 = (bf16[128,64]{0,1:T(8,128)(2,1)S(1)}, bf16[128,64]{0,1:T(8,128)(2,1)S(1)}, u32[]{:S(2)}, u32[]{:S(2)}) collective-permute-start(bf16[128,64]{0,1:T(8,128)(2,1)S(1)} %collective-permute-done.8), channel_id=1, source_target_pairs={{0,15},{1,0},{2,1},{3,2},{4,3},{5,4},{6,5},{7,6},{8,7},{9,8},{10,9... | collective-permute-start | bytes 49160 | tf_op jit(solution)/shard_map/ppermute | solution.py:21
  136.0 65.1 %copy-start.8 = (bf16[128,64]{0,1:T(8,128)(2,1)}, bf16[128,64]{0,1:T(8,128)(2,1)S(1)}, u32[]{:S(2)}) copy-start(bf16[128,64]{0,1:T(8,128)(2,1)S(1)} %collective-permute-done.2) | copy-start | bytes 49156
  136.0 16.6 %collective-permute-start.3 = (bf16[128,64]{0,1:T(8,128)(2,1)S(1)}, bf16[128,64]{0,1:T(8,128)(2,1)S(1)}, u32[]{:S(2)}, u32[]{:S(2)}) collective-permute-start(bf16[128,64]{0,1:T(8,128)(2,1)S(1)} %collective-permute-done.2), channel_id=1, source_target_pairs={{0,1},{1,2},{2,3},{3,4},{4,5},{5,6},{6,7},{7,8},{8,9},{9,10},{10,1... | collective-permute-start | bytes 49160 | tf_op jit(solution)/shard_map/ppermute | solution.py:19
  139.7 37.1 %copy-start.30 = (f32[128,2]{0,1:T(2,128)S(1)}, f32[128,2]{0,1:T(2,128)}, u32[]{:S(2)}) copy-start(f32[128,2]{0,1:T(2,128)} %param.28) | copy-start | bytes 3076
  139.7 61.5 %all-to-all-start.1 = ((bf16[16,32,1,16,128]{4,3,1,2,0:T(8,128)(2,1)}), bf16[16,32,1,16,128]{4,3,1,2,0:T(8,128)(2,1)S(1)}, u32[]{:S(2)}, u32[]{:S(2)}) async-start(bf16[16,32,1,16,128]{4,3,1,2,0:T(8,128)(2,1)} %broadcast_in_dim.22), calls=%async_computation.1 | async-start | bytes 4194304 | tf_op jit(solution)/shard_map/all_to_all | solution.py:41
  146.0 59.0 %copy-start.6 = (bf16[128,64]{0,1:T(8,128)(2,1)}, bf16[128,64]{0,1:T(8,128)(2,1)S(1)}, u32[]{:S(2)}) copy-start(bf16[128,64]{0,1:T(8,128)(2,1)S(1)} %collective-permute-done.9) | copy-start | bytes 49156
  146.0 22.1 %collective-permute-start.10 = (bf16[128,64]{0,1:T(8,128)(2,1)S(1)}, bf16[128,64]{0,1:T(8,128)(2,1)S(1)}, u32[]{:S(2)}, u32[]{:S(2)}) collective-permute-start(bf16[128,64]{0,1:T(8,128)(2,1)S(1)} %collective-permute-done.9), channel_id=1, source_target_pairs={{0,15},{1,0},{2,1},{3,2},{4,3},{5,4},{6,5},{7,6},{8,7},{9,8},{10,9... | collective-permute-start | bytes 49160 | tf_op jit(solution)/shard_map/ppermute | solution.py:21
  152.6 52.4 %copy-start.10 = (bf16[128,64]{0,1:T(8,128)(2,1)}, bf16[128,64]{0,1:T(8,128)(2,1)S(1)}, u32[]{:S(2)}) copy-start(bf16[128,64]{0,1:T(8,128)(2,1)S(1)} %collective-permute-done.3) | copy-start | bytes 49156
  152.6 22.2 %collective-permute-start.4 = (bf16[128,64]{0,1:T(8,128)(2,1)S(1)}, bf16[128,64]{0,1:T(8,128)(2,1)S(1)}, u32[]{:S(2)}, u32[]{:S(2)}) collective-permute-start(bf16[128,64]{0,1:T(8,128)(2,1)S(1)} %collective-permute-done.3), channel_id=1, source_target_pairs={{0,1},{1,2},{2,3},{3,4},{4,5},{5,6},{6,7},{7,8},{8,9},{9,10},{10,1... | collective-permute-start | bytes 49160 | tf_op jit(solution)/shard_map/ppermute | solution.py:19
  168.1 36.9 %copy-start.12 = (bf16[128,64]{0,1:T(8,128)(2,1)}, bf16[128,64]{0,1:T(8,128)(2,1)S(1)}, u32[]{:S(2)}) copy-start(bf16[128,64]{0,1:T(8,128)(2,1)S(1)} %collective-permute-done.10) | copy-start | bytes 49156
  168.1 8.7 %collective-permute-start.11 = (bf16[128,64]{0,1:T(8,128)(2,1)S(1)}, bf16[128,64]{0,1:T(8,128)(2,1)S(1)}, u32[]{:S(2)}, u32[]{:S(2)}) collective-permute-start(bf16[128,64]{0,1:T(8,128)(2,1)S(1)} %collective-permute-done.10), channel_id=1, source_target_pairs={{0,15},{1,0},{2,1},{3,2},{4,3},{5,4},{6,5},{7,6},{8,7},{9,8},{10,9... | collective-permute-start | bytes 49160 | tf_op jit(solution)/shard_map/ppermute | solution.py:21
  174.9 30.1 %copy-start.19 = (bf16[128,64]{0,1:T(8,128)(2,1)}, bf16[128,64]{0,1:T(8,128)(2,1)S(1)}, u32[]{:S(2)}) copy-start(bf16[128,64]{0,1:T(8,128)(2,1)S(1)} %collective-permute-done.4) | copy-start | bytes 49156
  174.9 8.7 %collective-permute-start.5 = (bf16[128,64]{0,1:T(8,128)(2,1)S(1)}, bf16[128,64]{0,1:T(8,128)(2,1)S(1)}, u32[]{:S(2)}, u32[]{:S(2)}) collective-permute-start(bf16[128,64]{0,1:T(8,128)(2,1)S(1)} %collective-permute-done.4), channel_id=1, source_target_pairs={{0,1},{1,2},{2,3},{3,4},{4,5},{5,6},{6,7},{7,8},{8,9},{9,10},{10,1... | collective-permute-start | bytes 49160 | tf_op jit(solution)/shard_map/ppermute | solution.py:19
  176.9 28.1 %copy-start.17 = (bf16[128,64]{0,1:T(8,128)(2,1)}, bf16[128,64]{0,1:T(8,128)(2,1)S(1)}, u32[]{:S(2)}) copy-start(bf16[128,64]{0,1:T(8,128)(2,1)S(1)} %collective-permute-done.11) | copy-start | bytes 49156
  176.9 8.7 %collective-permute-start.12 = (bf16[128,64]{0,1:T(8,128)(2,1)S(1)}, bf16[128,64]{0,1:T(8,128)(2,1)S(1)}, u32[]{:S(2)}, u32[]{:S(2)}) collective-permute-start(bf16[128,64]{0,1:T(8,128)(2,1)S(1)} %collective-permute-done.11), channel_id=1, source_target_pairs={{0,15},{1,0},{2,1},{3,2},{4,3},{5,4},{6,5},{7,6},{8,7},{9,8},{10,9... | collective-permute-start | bytes 49160 | tf_op jit(solution)/shard_map/ppermute | solution.py:21
  183.6 21.4 %copy-start.21 = (bf16[128,64]{0,1:T(8,128)(2,1)}, bf16[128,64]{0,1:T(8,128)(2,1)S(1)}, u32[]{:S(2)}) copy-start(bf16[128,64]{0,1:T(8,128)(2,1)S(1)} %collective-permute-done.5) | copy-start | bytes 49156
  183.6 8.7 %collective-permute-start.6 = (bf16[128,64]{0,1:T(8,128)(2,1)S(1)}, bf16[128,64]{0,1:T(8,128)(2,1)S(1)}, u32[]{:S(2)}, u32[]{:S(2)}) collective-permute-start(bf16[128,64]{0,1:T(8,128)(2,1)S(1)} %collective-permute-done.5), channel_id=1, source_target_pairs={{0,1},{1,2},{2,3},{3,4},{4,5},{5,6},{6,7},{7,8},{8,9},{9,10},{10,1... | collective-permute-start | bytes 49160 | tf_op jit(solution)/shard_map/ppermute | solution.py:19
  185.5 19.5 %copy-start.14 = (bf16[128,64]{0,1:T(8,128)(2,1)}, bf16[128,64]{0,1:T(8,128)(2,1)S(1)}, u32[]{:S(2)}) copy-start(bf16[128,64]{0,1:T(8,128)(2,1)S(1)} %collective-permute-done.12) | copy-start | bytes 49156
  185.6 8.8 %collective-permute-start.13 = (bf16[128,64]{0,1:T(8,128)(2,1)S(1)}, bf16[128,64]{0,1:T(8,128)(2,1)}, u32[]{:S(2)}, u32[]{:S(2)}) collective-permute-start(bf16[128,64]{0,1:T(8,128)(2,1)S(1)} %collective-permute-done.12), channel_id=1, source_target_pairs={{0,15},{1,0},{2,1},{3,2},{4,3},{5,4},{6,5},{7,6},{8,7},{9,8},{10,9... | collective-permute-start | bytes 49160 | tf_op jit(solution)/shard_map/ppermute | solution.py:21
  192.3 12.8 %copy-start.23 = (bf16[128,64]{0,1:T(8,128)(2,1)}, bf16[128,64]{0,1:T(8,128)(2,1)S(1)}, u32[]{:S(2)}) copy-start(bf16[128,64]{0,1:T(8,128)(2,1)S(1)} %collective-permute-done.6) | copy-start | bytes 49156
  192.3 8.8 %collective-permute-start.7 = (bf16[128,64]{0,1:T(8,128)(2,1)S(1)}, bf16[128,64]{0,1:T(8,128)(2,1)S(1)}, u32[]{:S(2)}, u32[]{:S(2)}) collective-permute-start(bf16[128,64]{0,1:T(8,128)(2,1)S(1)} %collective-permute-done.6), channel_id=1, source_target_pairs={{0,1},{1,2},{2,3},{3,4},{4,5},{5,6},{6,7},{7,8},{8,9},{9,10},{10,1... | collective-permute-start | bytes 49160 | tf_op jit(solution)/shard_map/ppermute | solution.py:19
  194.4 21.8 %collective-permute-start.14 = (bf16[128,64]{0,1:T(8,128)(2,1)}, bf16[128,64]{0,1:T(8,128)(2,1)}, u32[]{:S(2)}, u32[]{:S(2)}) collective-permute-start(bf16[128,64]{0,1:T(8,128)(2,1)} %collective-permute-done.13), channel_id=1, source_target_pairs={{0,15},{1,0},{2,1},{3,2},{4,3},{5,4},{6,5},{7,6},{8,7},{9,8},{10,9... | collective-permute-start | bytes 49160 | tf_op jit(solution)/shard_map/ppermute | solution.py:21
  211.4 5.5 %copy-start.26 = (bf16[128,64]{0,1:T(8,128)(2,1)S(1)}, bf16[128,64]{0,1:T(8,128)(2,1)}, u32[]{:S(2)}) copy-start(bf16[128,64]{0,1:T(8,128)(2,1)} %copy-done.25) | copy-start | bytes 49156
  211.4 5.5 %copy-start.24 = (bf16[128,64]{0,1:T(8,128)(2,1)S(1)}, bf16[128,64]{0,1:T(8,128)(2,1)}, u32[]{:S(2)}) copy-start(bf16[128,64]{0,1:T(8,128)(2,1)} %copy-done.23) | copy-start | bytes 49156
  211.4 5.5 %copy-start.22 = (bf16[128,64]{0,1:T(8,128)(2,1)S(1)}, bf16[128,64]{0,1:T(8,128)(2,1)}, u32[]{:S(2)}) copy-start(bf16[128,64]{0,1:T(8,128)(2,1)} %copy-done.21) | copy-start | bytes 49156
  211.4 5.5 %copy-start.20 = (bf16[128,64]{0,1:T(8,128)(2,1)S(1)}, bf16[128,64]{0,1:T(8,128)(2,1)}, u32[]{:S(2)}) copy-start(bf16[128,64]{0,1:T(8,128)(2,1)} %copy-done.19) | copy-start | bytes 49156
  211.4 5.5 %copy-start.11 = (bf16[128,64]{0,1:T(8,128)(2,1)S(1)}, bf16[128,64]{0,1:T(8,128)(2,1)}, u32[]{:S(2)}) copy-start(bf16[128,64]{0,1:T(8,128)(2,1)} %copy-done.10) | copy-start | bytes 49156
  211.4 5.5 %copy-start.9 = (bf16[128,64]{0,1:T(8,128)(2,1)S(1)}, bf16[128,64]{0,1:T(8,128)(2,1)}, u32[]{:S(2)}) copy-start(bf16[128,64]{0,1:T(8,128)(2,1)} %copy-done.8) | copy-start | bytes 49156
  211.4 5.6 %copy-start.7 = (bf16[128,64]{0,1:T(8,128)(2,1)S(1)}, bf16[128,64]{0,1:T(8,128)(2,1)}, u32[]{:S(2)}) copy-start(bf16[128,64]{0,1:T(8,128)(2,1)} %copy-done.6) | copy-start | bytes 49156
  211.5 27.9 %all-to-all-start.2 = ((bf16[16,32,1,16,128]{4,3,1,2,0:T(8,128)(2,1)}), bf16[16,32,1,16,128]{4,3,1,2,0:T(8,128)(2,1)S(1)}, u32[]{:S(2)}, u32[]{:S(2)}) async-start(bf16[16,32,1,16,128]{4,3,1,2,0:T(8,128)(2,1)} %broadcast_in_dim.23), calls=%async_computation.2 | async-start | bytes 4194304 | tf_op jit(solution)/shard_map/all_to_all | solution.py:41
  217.1 22.3 %copy-start.5 = (bf16[128,2048]{0,1:T(8,128)(2,1)}, bf16[128,2048]{0,1:T(8,128)(2,1)S(1)}, u32[]{:S(2)}) copy-start(bf16[128,2048]{0,1:T(8,128)(2,1)S(1)} %constant_dynamic-update-slice_fusion.3) | copy-start | bytes 1572868
  246.0 17.0 %copy-start.16 = (bf16[128,64]{0,1:T(8,128)(2,1)S(1)}, bf16[128,64]{0,1:T(8,128)(2,1)}, u32[]{:S(2)}) copy-start(bf16[128,64]{0,1:T(8,128)(2,1)} %copy-done.14) | copy-start | bytes 49156
  246.0 20.2 %copy-start.4 = (bf16[1024,128]{1,0:T(8,128)(2,1)S(1)}, bf16[1024,128]{1,0:T(8,128)(2,1)}, u32[]{:S(2)}) copy-start(bf16[1024,128]{1,0:T(8,128)(2,1)} %param.23) | copy-start | bytes 786436
  247.4 31.4 %all-to-all-start.3 = ((bf16[32,1,16,128]{3,2,1,0:T(8,128)(2,1)}), bf16[32,1,16,128]{3,2,1,0:T(8,128)(2,1)S(1)}, u32[]{:S(2)}, u32[]{:S(2)}) async-start(bf16[32,1,16,128]{3,2,1,0:T(8,128)(2,1)} %fusion.22), calls=%async_computation.3 | async-start | bytes 262144 | tf_op jit(solution)/shard_map/all_to_all | solution.py:156
  (6 other events, 19.8 us)
Sparse Core Ops, SparseCore 0:
  12.4 77.6 all-gather.1
